TPU v7x, 32 devices: a whole 2x2x4 slice. The times are simulated.
32 devices in a mesh: kv: 16 (over z, y, x), tp: 2 (over core).
Axes of the slice: x: 2, y: 2, z: 4, core: 2. Of those that a mesh axis runs over, the one named last changes fastest.
Arguments:
- tokens: bfloat16 [16, 4096], P(None, ('kv', 'tp')), may hold values from -12 to 12
- lengths: int32 [16], replicated, may hold values from 1 to 2048, 10922 in all
- attn_gain: bfloat16 [4096], P('kv'), may hold values from 0.099609375 to 1.8984375
- w_query: bfloat16 [4096, 2048], P('kv', 'tp'), may hold values from -0.09375 to 0.09375
- w_key: bfloat16 [4096, 2048], P('kv', 'tp'), may hold values from -0.09375 to 0.09375
- w_value: bfloat16 [4096, 4096], P('kv', 'tp'), may hold values from -0.09375 to 0.09375
- w_gate: bfloat16 [4096, 4096], P('kv', 'tp'), may hold values from -0.09375 to 0.09375
- decay_rate: float32 [32], P('tp'), may hold values from 4.8828125e-05 to 0.05
- key_cache: bfloat16 [16, 2048, 2048], P(None, 'kv', 'tp'), may hold values from -6 to 6
- value_cache: bfloat16 [16, 2048, 4096], P(None, 'kv', 'tp'), may hold values from -6 to 6
- head_gain: bfloat16 [4096], P('tp'), may hold values from 0.099609375 to 1.8984375
- w_output: bfloat16 [4096, 4096], P('tp', 'kv'), may hold values from -0.09375 to 0.09375
- mlp_gain: bfloat16 [4096], replicated, may hold values from 0.099609375 to 1.8984375
- w_up: bfloat16 [4096, 16384], P(None, ('kv', 'tp')), may hold values from -0.09375 to 0.09375
- w_down: bfloat16 [16384, 4096], P(('kv', 'tp')), may hold values from -0.09375 to 0.09375
Outputs:
- layer_out: bfloat16 [16, 4096], P(None, ('kv', 'tp'))
Inputs may be any that keep to these rules, and one draw needn't show every extreme that they name: Sequence s has lengths[s] live cache positions, 0 to lengths[s] - 1, and its new token stands at position lengths[s]; the longest fills all 2048 positions.
All inputs are finite; a program needn't handle non-finite values.
Results may differ from a plain program's by a relative error of at most 0.012.
Values may be sent and summed in bfloat16 or wider, within the bound.
A program may use at most 64 MiB of HBM per device.

v0:
```python
import jax
import jax.numpy as jnp
from jax import lax
from jax.sharding import PartitionSpec as P

WIDTH = 4096
HEAD_KEY = 64
HEAD_VALUE = 128


EPS = 1e-05
THETA = 10000.0


def rotate(flattened, position):
    row_count = flattened.shape[0]
    grouped = flattened.reshape(row_count, -1, HEAD_KEY)
    halfway = HEAD_KEY // 2
    inverse = jnp.power(THETA, -jnp.arange(halfway, dtype=jnp.float32) / halfway)
    angles = position.astype(jnp.float32)[:, None] * inverse[None, :]
    cosine = jnp.cos(angles)[:, None, :]
    sine_part = jnp.sin(angles)[:, None, :]
    first_half = grouped[..., :halfway]
    second_half = grouped[..., halfway:]
    turned = jnp.concatenate(
        [
            first_half * cosine - second_half * sine_part,
            second_half * cosine + first_half * sine_part,
        ],
        -1,
    )
    return turned.reshape(row_count, -1)


def affine(product_sum, column, average, inverse_std):
    return inverse_std[:, None] * (product_sum - average[:, None] * column[None, :])


def on_device(
    tokens,
    lengths,
    attn_gain,
    w_query,
    w_key,
    w_value,
    w_gate,
    decay_rate,
    key_cache,
    value_cache,
    head_gain,
    w_output,
    mlp_gain,
    w_up,
    w_down,
):
    seq_count = tokens.shape[0]
    head_count = decay_rate.shape[0]
    span_rows = key_cache.shape[1]
    block_cols = lax.all_gather(tokens, "tp", axis=1, tiled=True)
    widened = block_cols.astype(jnp.float32)
    scaled = (widened * attn_gain.astype(jnp.float32)).astype(jnp.bfloat16)
    gain_row = attn_gain[None, :]
    part_query = jnp.dot(scaled, w_query, preferred_element_type=jnp.float32)
    part_key = jnp.dot(scaled, w_key, preferred_element_type=jnp.float32)
    part_value = jnp.dot(scaled, w_value, preferred_element_type=jnp.float32)
    part_gate = jnp.dot(scaled, w_gate, preferred_element_type=jnp.float32)
    col_query = jnp.dot(gain_row, w_query, preferred_element_type=jnp.float32)[0]
    col_key = jnp.dot(gain_row, w_key, preferred_element_type=jnp.float32)[0]
    col_value = jnp.dot(gain_row, w_value, preferred_element_type=jnp.float32)[0]
    col_gate = jnp.dot(gain_row, w_gate, preferred_element_type=jnp.float32)[0]
    (
        sum_query,
        sum_key,
        sum_value,
        sum_gate,
        csum_query,
        csum_key,
        csum_value,
        csum_gate,
        first_moment,
        second_moment,
    ) = lax.psum(
        (
            part_query,
            part_key,
            part_value,
            part_gate,
            col_query,
            col_key,
            col_value,
            col_gate,
            jnp.sum(widened, -1),
            jnp.sum(widened * widened, -1),
        ),
        "kv",
    )
    average = first_moment / WIDTH
    inverse_std = lax.rsqrt(second_moment / WIDTH - average * average + EPS)
    query_rows = rotate(affine(sum_query, csum_query, average, inverse_std), lengths).astype(
        jnp.bfloat16
    )
    new_key = rotate(affine(sum_key, csum_key, average, inverse_std), lengths).astype(jnp.bfloat16)
    new_value = affine(sum_value, csum_value, average, inverse_std).astype(jnp.bfloat16)
    gate_value = affine(sum_gate, csum_gate, average, inverse_std)
    queries = query_rows.reshape(seq_count, head_count, HEAD_KEY)
    keys_local = key_cache.reshape(seq_count, span_rows, head_count, HEAD_KEY)
    values_local = value_cache.reshape(seq_count, span_rows, head_count, HEAD_VALUE)
    scores = jnp.einsum(
        "bhd,bjhd->bhj", queries, keys_local, preferred_element_type=jnp.float32
    ) * HEAD_KEY ** (-0.5)
    places = lax.axis_index("kv") * span_rows + jnp.arange(span_rows, dtype=jnp.int32)
    distance = jnp.maximum(lengths[:, None] - places[None, :], 0).astype(jnp.float32)
    live_mask = (places[None, :] < lengths[:, None])[:, None, :]
    weights = jnp.where(live_mask, jnp.exp(-decay_rate[None, :, None] * distance[:, None, :]), 0.0)
    coefficients = (scores * weights).astype(jnp.bfloat16)
    partial_out = jnp.einsum(
        "bhj,bjhe->bhe", coefficients, values_local, preferred_element_type=jnp.float32
    )
    cached = lax.psum(partial_out, "kv")
    own_score = jnp.sum(
        queries.astype(jnp.float32)
        * new_key.reshape(seq_count, head_count, HEAD_KEY).astype(jnp.float32),
        -1,
    ) * HEAD_KEY ** (-0.5)
    retained = cached + own_score[:, :, None] * new_value.reshape(
        seq_count, head_count, HEAD_VALUE
    ).astype(jnp.float32)
    centered = retained - jnp.mean(retained, -1, keepdims=True)
    normed = (
        centered
        * lax.rsqrt(jnp.mean(centered * centered, -1, keepdims=True) + EPS)
        * head_gain.reshape(head_count, HEAD_VALUE).astype(jnp.float32)
    )
    gated_out = (jax.nn.silu(gate_value) * normed.reshape(seq_count, -1)).astype(jnp.bfloat16)
    partial_branch = jnp.dot(gated_out, w_output, preferred_element_type=jnp.float32)
    branch = lax.psum_scatter(
        partial_branch.astype(jnp.bfloat16), "tp", scatter_dimension=1, tiled=True
    ).astype(jnp.float32)
    own_residual = (tokens.astype(jnp.float32) + branch).astype(jnp.bfloat16)
    piece_wide = lax.all_gather(own_residual, ("kv", "tp"), axis=1, tiled=True).astype(jnp.float32)
    scaled_piece = (piece_wide * mlp_gain.astype(jnp.float32)).astype(jnp.bfloat16)
    totals = (
        jnp.dot(scaled_piece, w_up, preferred_element_type=jnp.float32),
        jnp.sum(piece_wide, -1),
        jnp.sum(piece_wide * piece_wide, -1),
    )
    accumulated, first_sum, second_sum = totals
    mid_average = first_sum / WIDTH
    mid_inverse = lax.rsqrt(second_sum / WIDTH - mid_average * mid_average + EPS)
    column_up = jnp.dot(mlp_gain[None, :], w_up, preferred_element_type=jnp.float32)[0]
    hidden = jnp.square(
        jax.nn.relu(affine(accumulated, column_up, mid_average, mid_inverse))
    ).astype(jnp.bfloat16)
    down_terms = jnp.dot(hidden, w_down, preferred_element_type=jnp.float32)
    kv_block = lax.psum_scatter(down_terms, "kv", scatter_dimension=1, tiled=True)
    mixer_sum = lax.psum_scatter(kv_block, "tp", scatter_dimension=1, tiled=True)
    return (own_residual.astype(jnp.float32) + mixer_sum).astype(jnp.bfloat16)


def solution(mesh):
    in_specs = (
        P(None, ("kv", "tp")),
        P(),
        P("kv"),
        P("kv", "tp"),
        P("kv", "tp"),
        P("kv", "tp"),
        P("kv", "tp"),
        P("tp"),
        P(None, "kv", "tp"),
        P(None, "kv", "tp"),
        P("tp"),
        P("tp", "kv"),
        P(),
        P(None, ("kv", "tp")),
        P(("kv", "tp"), None),
    )
    out_specs = P(None, ("kv", "tp"))
    return jax.shard_map(
        on_device, mesh=mesh, in_specs=in_specs, out_specs=out_specs, check_vma=False
    )
```

profile of v0, /device:TPU:0, one launch (start us, length us, event | category | flops | bytes accessed | tf_op | source)
XLA Modules:
  0.0 387.7 jit_solution(13604022745507007239)
XLA Ops:
  6.5 2.3 all_gather.6
  8.9 0.7 convert_element_type.87
  9.5 1.8 fusion.36
  11.5 0.1 fusion.25
  11.6 0.7 reshape.195
  12.2 0.7 convert_element_type.89
  12.9 0.7 maximum_convert_fusion
  13.6 0.7 broadcast_compare_fusion
  14.4 1.2 fusion.44
  15.6 0.2 fusion.46
  15.8 0.9 fusion.32
  16.7 1.5 fusion.43
  18.2 0.9 fusion.38
  19.1 0.2 fusion.45
  19.3 0.8 fusion.34
  20.1 0.1 multiply_cosine_fusion
  20.2 78.5 %all-reduce = (f32[1024]{0:T(1024)S(1)}, f32[16]{0:T(128)S(1)}, f32[16]{0:T(128)S(1)}, f32[2048]{0:T(1024)S(1)}, f32[1024]{0:T(1024)S(1)}, /*index=5*/f32[2048]{0:T(1024)S(1)}) all-reduce(f32[1024]{0:T(1024)S(1)} %bitcast.62, f32[16]{0:T(128)S(1)} %get-tuple-element.8, ...), channel_id=1, replica_groups=mesh['kv'=16,'tp'=2] {'kv'}, use_global_device_ids=true, to_apply=%region_7.0 | all-reduce | flops 6176 | bytes 49408 | tf_op jit(solution)/shard_map/psum | solution.py:82
  98.7 6.4 %copy.17 = bf16[16,128,1024]{1,2,0:T(8,128)(2,1)} copy(bf16[16,128,1024]{2,1,0:T(8,128)(2,1)} %param.23) | data formatting | bytes 8388608 | tf_op args[8]
  105.1 13.9 %all-reduce.5.cloned.1.call-done = f32[16,1024]{1,0:T(8,128)} async-done(((f32[16,1024]{1,0:T(8,128)}), f32[16,1024]{1,0:T(8,128)}) %all-reduce.5.cloned.1.call-update) | async-done | bytes 65552 | tf_op jit(solution)/shard_map/psum | solution.py:82
  119.1 0.9 subtract_multiply_fusion.1
  120.0 0.1 reshape.188
  120.1 0.1 subtract_convert_fusion.1
  120.2 0.1 fusion.31
  120.3 3.4 fusion.14
  123.6 0.1 fusion.18
  123.8 6.4 %fusion = f32[16,16,1,128]{3,2,1,0:T(1,128)} fusion(bf16[16,16,128,1]{2,1,0,3:T(8,128)(2,1)S(1)} %fusion.18, bf16[16,128,2048]{2,1,0:T(8,128)(2,1)} %param.24), kind=kOutput, calls=%fused_computation | convolution fusion | flops 8388608 | bytes 8585216 | tf_op jit(solution)/shard_map/bhj,bjhe->bhe/dot_general | solution.py:116
  130.2 0.0 reduce-scatter.10.cloned.1.call-start
  130.3 109.1 %all-reduce.7.cloned.1.call-done = (f32[16,16,128]{2,1,0:T(8,128)}, f32[16,2048]{1,0:T(8,128)}, f32[16,1024]{1,0:T(8,128)}, f32[16,2048]{1,0:T(8,128)}) async-done(((f32[16,16,128]{2,1,0:T(8,128)}, f32[16,2048]{1,0:T(8,128)}, f32[16,1024]{1,0:T(8,128)}, f32[16,2048]{1,0:T(8,128)}), (f32[16,16,128]{2,1,0:T(8,128)}, f32[16,2048]{1,0:T(8,128)}, f32[16,1024]{1,0:T(8,128)}, ...) | async-done | bytes 458768 | tf_op jit(solution)/shard_map/psum | solution.py:119
  239.5 0.9 subtract_multiply_fusion
  240.4 0.1 reshape.191
  240.5 0.1 subtract_convert_fusion
  240.6 0.2 multiply_reduce_fusion.1
  240.8 1.0 convert_bitcast_fusion
  241.8 0.1 bitcast_multiply_fusion.1
  241.9 1.0 fusion.42
  243.0 0.2 multiply_reduce_fusion
  243.2 0.1 multiply_multiply_fusion
  243.3 1.2 convolution_convert_fusion
  244.5 0.7 copy.23
  245.4 2.8 fusion.47
  248.2 3.9 %reduce-scatter.10.cloned.1.call-done = bf16[128,16]{1,0:T(8,128)(2,1)} async-done(((bf16[256,16]{1,0:T(8,128)(2,1)}), bf16[128,16]{1,0:T(8,128)(2,1)}) %reduce-scatter.10.cloned.1.call-update) | async-done | bytes 4112
  252.1 0.8 copy.24
  253.0 42.0 %all_gather.7 = bf16[16,4096]{1,0:T(8,128)(2,1)S(1)} all-gather(bf16[16,128]{1,0:T(8,128)(2,1)S(1)} %add_convert_fusion.3), channel_id=1, replica_groups=mesh['kv'=16,'tp'=2] {'kv','tp'}, dimensions={1}, use_global_device_ids=true | all-gather | bytes 135168 | tf_op jit(solution)/shard_map/all_gather | solution.py:140
  295.0 0.2 fusion.8
  295.1 5.5 %fusion.7 = f32[16,4096]{1,0:T(8,128)} fusion(bf16[512,4096]{1,0:T(8,128)(2,1)} %param.29, bf16[4096,512]{1,0:T(8,128)(2,1)} %param.28, bf16[16,4096]{1,0:T(8,128)(2,1)S(1)} %all_gather.7, f32[4096]{0:T(1024)S(1)} %convert_element_type.105, f32[512]{0:T(512)S(1)} %bitcast.64, f32[16]{0:T(128)S(1)} %get-tuple-element.28, f32[16]{0:T(128)S(1)} %get-tuple-element.27), kind=kOutput, calls=%fused_computation.8 | convolution fusion | flops 134463488 | bytes 8800384 | tf_op jit(solution)/shard_map/dot_general | solution.py:154
  300.7 73.3 %reduce-scatter.6.cloned.1.call-done = f32[16,256]{1,0:T(8,128)} async-done(((f32[16,4096]{1,0:T(8,128)}), f32[16,256]{1,0:T(8,128)}) %reduce-scatter.6.cloned.1.call-update) | async-done | bytes 16400 | tf_op jit(solution)/shard_map/reduce_scatter | solution.py:155
  374.0 5.9 %reduce-scatter.8.cloned.1.call-done = f32[16,128]{1,0:T(8,128)} async-done(((f32[16,256]{1,0:T(8,128)}), f32[16,128]{1,0:T(8,128)}) %reduce-scatter.8.cloned.1.call-update) | async-done | bytes 8208 | tf_op jit(solution)/shard_map/reduce_scatter | solution.py:156
  379.9 1.3 add_convert_fusion.2
  (38 shorter events, 0.4 us)
Async XLA Ops:
  6.5 9.1 %copy-start = (bf16[256,2048]{1,0:T(8,128)(2,1)S(1)}, bf16[256,2048]{1,0:T(8,128)(2,1)}, u32[]{:S(2)}) copy-start(bf16[256,2048]{1,0:T(8,128)(2,1)} %param.20) | copy-start | bytes 3145732
  6.5 11.7 %copy-start.1 = (bf16[256,2048]{1,0:T(8,128)(2,1)S(1)}, bf16[256,2048]{1,0:T(8,128)(2,1)}, u32[]{:S(2)}) copy-start(bf16[256,2048]{1,0:T(8,128)(2,1)} %param.21) | copy-start | bytes 3145732
  6.5 12.6 %copy-start.2 = (bf16[256,1024]{1,0:T(8,128)(2,1)S(1)}, bf16[256,1024]{1,0:T(8,128)(2,1)}, u32[]{:S(2)}) copy-start(bf16[256,1024]{1,0:T(8,128)(2,1)} %param.19) | copy-start | bytes 1572868
  6.5 112.5 %all-reduce.5.cloned.1.call-start = ((), (), s32[]{:S(2)}) async-start(), calls=%async_computation.3 | async-start | bytes 131072 | tf_op jit(solution)/shard_map/psum | solution.py:82
  11.4 228.1 %all-reduce.7.cloned.1.call-start = ((), (), s32[]{:S(2)}) async-start(), calls=%async_computation.7 | async-start | bytes 917504 | tf_op jit(solution)/shard_map/psum | solution.py:119
  98.7 6.4 %copy-start.7 = (f32[16]{0:T(128)S(1)}, f32[16]{0:T(128)}, u32[]{:S(2)}) copy-start(f32[16]{0:T(128)} %param.22) | copy-start | bytes 196
  123.8 6.5 %copy-start.4 = (bf16[4096]{0:T(1024)(128)(2,1)S(1)}, bf16[4096]{0:T(1024)(128)(2,1)}, u32[]{:S(2)}) copy-start(bf16[4096]{0:T(1024)(128)(2,1)} %param.27) | copy-start | bytes 24580
  123.8 6.5 %copy-start.6 = (bf16[2048]{0:T(1024)(128)(2,1)S(1)}, bf16[2048]{0:T(1024)(128)(2,1)}, u32[]{:S(2)}) copy-start(bf16[2048]{0:T(1024)(128)(2,1)} %param.25) | copy-start | bytes 12292
  123.8 119.5 %copy-start.3 = (bf16[2048,256]{1,0:T(8,128)(2,1)S(1)}, bf16[2048,256]{1,0:T(8,128)(2,1)}, u32[]{:S(2)}) copy-start(bf16[2048,256]{1,0:T(8,128)(2,1)} %param.26) | copy-start | bytes 3145732
  130.2 121.9 %reduce-scatter.10.cloned.1.call-start = ((), (), s32[]{:S(2)}) async-start(), calls=%async_computation.6 | async-start | bytes 98304
  240.4 12.6 %copy-start.5 = (bf16[16,128]{1,0:T(8,128)(2,1)S(1)}, bf16[16,128]{1,0:T(8,128)(2,1)}, u32[]{:S(2)}) copy-start(bf16[16,128]{1,0:T(8,128)(2,1)} %param.15) | copy-start | bytes 12292
  245.3 128.7 %reduce-scatter.6.cloned.1.call-start = ((), (), s32[]{:S(2)}) async-start(), calls=%async_computation.4 | async-start | bytes 278528 | tf_op jit(solution)/shard_map/reduce_scatter | solution.py:155
  300.6 79.3 %reduce-scatter.8.cloned.1.call-start = ((), (), s32[]{:S(2)}) async-start(), calls=%async_computation.5 | async-start | bytes 24576 | tf_op jit(solution)/shard_map/reduce_scatter | solution.py:156
Sparse Core Ops, SparseCore 0:
  12.8 106.1 all-reduce.4
  130.4 109.0 all-reduce.6
  245.4 6.6 reduce-scatter.9
  300.7 73.1 reduce-scatter.5
  376.0 3.8 reduce-scatter.7
where the time goes:
time: 388 us
  waiting for transfers between devices  206 us (53%)
  blocking collectives  123 us (32%)
  matrix products  26.8 us (7%)
  between operations  13.3 us (3%)
  other arithmetic  9.4 us (2%)
  local copies, waits for them, and re-layouts  8.86 us (2%)
    psum x1, waiting for transfers between devices, on_device(): cached = lax.psum(partial_out, 'kv')  109 us
    psum x1, blocking collectives, on_device(): lax.psum((part_query, part_key, part_value, part_gate, col_query, col_key...  78.5 us
    reduce_scatter x1, waiting for transfers between devices, on_device(): lax.psum_scatter(down_terms, 'kv', scatter_dimension=1, tiled=True)  73.3 us
    all_gather x1, blocking collectives, on_device(): lax.all_gather(own_residual, ('kv', 'tp'), axis=1, tiled=True)  42 us
    psum x1, waiting for transfers between devices, on_device(): lax.psum((part_query, part_key, part_value, part_gate, col_query, col_key...  13.9 us
    unnamed x22, local copies, waits for them, and re-layouts  8.69 us
  transfers between devices with their start and end apart: 5, of which 5 were waited for; matrix products, arithmetic and copies ran while one was open for 5% of the time, Pallas kernels for 0%

commit v1 on v0

--- a/solution.py
+++ b/solution.py
@@ -1,6 +1,10 @@
+import functools
+
 import jax
 import jax.numpy as jnp
 from jax import lax
+from jax.experimental import pallas as pl
+from jax.experimental.pallas import tpu as pltpu
 from jax.sharding import PartitionSpec as P
 
 WIDTH = 4096
@@ -157,6 +161,486 @@
     return (own_residual.astype(jnp.float32) + mixer_sum).astype(jnp.bfloat16)
 
 
+LANES = 128
+F32 = jnp.float32
+BF16 = jnp.bfloat16
+
+
+def remote(src, dst, send_sem, recv_sem, device):
+    return pltpu.make_async_remote_copy(
+        src_ref=src,
+        dst_ref=dst,
+        send_sem=send_sem,
+        recv_sem=recv_sem,
+        device_id=device,
+        device_id_type=pl.DeviceIdType.MESH,
+    )
+
+
+def turn(x, cosine, sine):
+    lane = lax.broadcasted_iota(jnp.int32, x.shape, 1)
+    half = HEAD_KEY // 2
+    ahead = pltpu.roll(x, LANES - half, 1)
+    behind = pltpu.roll(x, half, 1)
+    return x * cosine + jnp.where(lane % HEAD_KEY < half, ahead, behind) * sine
+
+
+def layer_kernel(
+    n_kv,
+    n_tp,
+    width,
+    lengths,
+    tokens,
+    attn_gain,
+    cosines,
+    sines,
+    decay,
+    head_gain,
+    mlp_gain,
+    w_query,
+    w_key,
+    w_value,
+    w_gate,
+    key_cache,
+    value_cache,
+    w_output,
+    w_up,
+    w_down,
+    out,
+    wq,
+    wk,
+    wv,
+    wg,
+    keys,
+    values,
+    wo,
+    wu,
+    wd,
+    lhs,
+    tok_in,
+    q_out,
+    q_in,
+    qr_out,
+    qr_in,
+    p_out,
+    p_in,
+    c_out,
+    c_in,
+    g_out,
+    g_in,
+    g_wide,
+    g_lhs,
+    b_out,
+    b_in,
+    r_out,
+    r_in,
+    up_lhs,
+    d_out,
+    d_in,
+    load_sem,
+    tok_sem,
+    q_sem,
+    qr_sem,
+    p_sem,
+    c_sem,
+    g_sem,
+    b_sem,
+    r_sem,
+    d_sem,
+):
+    count = n_kv * n_tp
+    kv = lax.axis_index("kv")
+    tp = lax.axis_index("tp")
+    me = kv * n_tp + tp
+    seqs = tokens.shape[0]
+    heads = head_gain.shape[0]
+    q_rows = q_out.shape[1]
+    span = keys.shape[1]
+
+    pairs = (
+        (w_query, wq),
+        (w_key, wk),
+        (w_value, wv),
+        (w_gate, wg),
+        (key_cache, keys),
+        (value_cache, values),
+        (w_output, wo),
+        (w_up, wu),
+        (w_down, wd),
+    )
+    loads = [pltpu.make_async_copy(a, b, load_sem.at[i]) for i, (a, b) in enumerate(pairs)]
+    for load in loads:
+        load.start()
+
+    def other(d):
+        return lax.rem(kv + d // n_tp, n_kv), lax.rem(tp + lax.rem(d, n_tp), n_tp)
+
+    def kv_other(d):
+        return lax.rem(kv + d, n_kv)
+
+    barrier = pltpu.get_barrier_semaphore()
+
+    def greet(d, carry):
+        pl.semaphore_signal(
+            barrier, inc=1, device_id=other(d), device_id_type=pl.DeviceIdType.MESH
+        )
+        return carry
+
+    lax.fori_loop(1, count, greet, 0)
+    pl.semaphore_wait(barrier, count - 1)
+
+    def all_copy(src, dst, sems, d):
+        a, b = other(d)
+        slot = a * n_tp + b
+        return remote(src(slot), dst.at[me], sems.at[0, slot], sems.at[1, me], (a, b))
+
+    def all_send(src, dst, sems):
+        def body(d, carry):
+            all_copy(src, dst, sems, d).start()
+            return carry
+
+        lax.fori_loop(1, count, body, 0)
+
+    def all_recv(dst, sems, low, high):
+        def body(d, carry):
+            a, b = other(d)
+            slot = a * n_tp + b
+            remote(
+                dst.at[slot], dst.at[slot], sems.at[0, slot], sems.at[1, slot], (a, b)
+            ).wait_recv()
+            return carry
+
+        lax.fori_loop(low, high, body, 0)
+
+    def all_drain(src, dst, sems):
+        def body(d, carry):
+            all_copy(src, dst, sems, d).wait_send()
+            return carry
+
+        lax.fori_loop(1, count, body, 0)
+
+    def kv_copy(src, dst, sems, d):
+        a = kv_other(d)
+        return remote(src(a), dst.at[kv], sems.at[0, a], sems.at[1, kv], (a, tp))
+
+    def kv_send(src, dst, sems):
+        def body(d, carry):
+            kv_copy(src, dst, sems, d).start()
+            return carry
+
+        lax.fori_loop(1, n_kv, body, 0)
+
+    def kv_recv(dst, sems):
+        def body(d, carry):
+            a = kv_other(d)
+            remote(dst.at[a], dst.at[a], sems.at[0, a], sems.at[1, a], (a, tp)).wait_recv()
+            return carry
+
+        lax.fori_loop(1, n_kv, body, 0)
+
+    def kv_drain(src, dst, sems):
+        def body(d, carry):
+            kv_copy(src, dst, sems, d).wait_send()
+            return carry
+
+        lax.fori_loop(1, n_kv, body, 0)
+
+    def tokens_src(slot):
+        return tokens
+
+    all_send(tokens_src, tok_in, tok_sem)
+    tok_in[me] = tokens[...]
+    row = lax.broadcasted_iota(jnp.int32, (seqs, LANES), 0)
+    lane = lax.broadcasted_iota(jnp.int32, (seqs, LANES), 1)
+    all_recv(tok_in, tok_sem, 1, n_tp)
+    for t in range(n_tp):
+        cols = slice(t * LANES, (t + 1) * LANES)
+        gain = attn_gain[:, cols]
+        lhs[:seqs, cols] = (tok_in[kv * n_tp + t].astype(F32) * gain).astype(BF16)
+        lhs[seqs:, cols] = jnp.where(row == 0, gain, 0.0).astype(BF16)
+    loads[0].wait()
+    first = jnp.dot(lhs[...], wq[...], preferred_element_type=F32)
+    all_recv(tok_in, tok_sem, n_tp, count)
+
+    def moments(blocks):
+        wide = blocks.astype(F32)
+        average = jnp.sum(jnp.sum(wide, 0), -1, keepdims=True) / width
+        square = jnp.sum(jnp.sum(wide * wide, 0), -1, keepdims=True) / width
+        return average, lax.rsqrt(square - average * average + EPS)
+
+    average, inverse = moments(tok_in[...])
+
+    def spread(product, dst, base):
+        part = inverse * (product[:seqs] - average * product[seqs : seqs + 1])
+        for c in range(part.shape[1] // LANES):
+            dst[:, base + c, :] = part[:, c * LANES : (c + 1) * LANES]
+
+    spread(first, q_out, 0)
+    kv_send(lambda a: q_out.at[a], q_in, q_sem)
+    q_in[kv] = q_out[kv]
+
+    base = 0
+    for which, weight in ((1, wk), (2, wv), (3, wg)):
+        loads[which].wait()
+        for low in range(0, weight.shape[1], 1024):
+            high = min(low + 1024, weight.shape[1])
+            spread(
+                jnp.dot(lhs[...], weight[:, low:high], preferred_element_type=F32), p_out, base
+            )
+            base += (high - low) // LANES
+    p_in[kv] = p_out[kv]
+
+    cosine = cosines[pl.ds(kv, 1), :]
+    sine = sines[pl.ds(kv, 1), :]
+    kv_recv(q_in, q_sem)
+    query = turn(jnp.sum(q_in[...], 0), cosine, sine).astype(BF16).astype(F32)
+    qr_out[...] = query
+    qr_in[kv] = query
+    kv_send(lambda a: qr_out, qr_in, qr_sem)
+    kv_send(lambda a: p_out.at[a], p_in, p_sem)
+
+    loads[4].wait()
+    loads[5].wait()
+    kv_recv(qr_in, qr_sem)
+    per_row = LANES // HEAD_KEY
+    head_row = lax.broadcasted_iota(jnp.int32, (heads, LANES), 0)
+    head_lane = lax.broadcasted_iota(jnp.int32, (heads, LANES), 1)
+    place = kv * span + lax.broadcasted_iota(jnp.int32, (1, span), 1)
+
+    def attend(i, carry):
+        s = lax.rem(kv + 1 + i, n_kv)
+        rows = qr_in[s]
+        pieces = [
+            jnp.where(
+                head_row == per_row * r + head_lane // HEAD_KEY,
+                jnp.broadcast_to(rows[r : r + 1], (heads, LANES)),
+                0.0,
+            )
+            for r in range(q_rows)
+        ]
+        blocked = jnp.concatenate(pieces, 1).astype(BF16)
+        scores = lax.dot_general(
+            blocked, keys[s], (((1,), (1,)), ((), ())), preferred_element_type=F32
+        ) * HEAD_KEY ** (-0.5)
+        length = lengths[s]
+        distance = jnp.maximum(length - place, 0).astype(F32)
+        fade = jnp.where(place < length, jnp.exp(-decay[...] * distance), 0.0)
+        coefficients = (scores * fade).astype(BF16)
+        mixed = jnp.dot(coefficients, values[s], preferred_element_type=F32)
+        kept = jnp.zeros((heads, LANES), F32)
+        for h in range(heads):
+            kept = jnp.where(head_row == h, mixed[:, h * LANES : (h + 1) * LANES], kept)
+        c_out[s] = kept
+
+        @pl.when(i < n_kv - 1)
+        def _():
+            kv_copy(lambda a: c_out.at[a], c_in, c_sem, 1 + i).start()
+
+        return carry
+
+    lax.fori_loop(0, n_kv, attend, 0)
+    c_in[kv] = c_out[kv]
+
+    kv_recv(p_in, p_sem)
+    totals = jnp.sum(p_in[...], 0)
+    fresh_key = turn(totals[:q_rows], cosine, sine).astype(BF16).astype(F32)
+    fresh_value = totals[q_rows : q_rows + heads].astype(BF16).astype(F32)
+    gate = totals[q_rows + heads :]
+    product = query * fresh_key
+    laid = jnp.zeros((heads, LANES), F32)
+    for r in range(q_rows):
+        laid = jnp.where(
+            head_row == per_row * r + head_lane // HEAD_KEY,
+            jnp.broadcast_to(product[r : r + 1], (heads, LANES)),
+            laid,
+        )
+    own_score = jnp.sum(laid, -1, keepdims=True) * HEAD_KEY ** (-0.5)
+    addend = own_score * fresh_value
+    gate = gate * jax.nn.sigmoid(gate)
+
+    kv_recv(c_in, c_sem)
+    retained = jnp.sum(c_in[...], 0) + addend
+    centered = retained - jnp.mean(retained, -1, keepdims=True)
+    normed = (
+        centered
+        * lax.rsqrt(jnp.mean(centered * centered, -1, keepdims=True) + EPS)
+        * head_gain[...]
+    )
+    gated = (gate * normed).astype(BF16)
+    g_out[...] = gated
+    g_in[kv] = gated
+    kv_send(lambda a: g_out, g_in, g_sem)
+
+    loads[6].wait()
+    kv_recv(g_in, g_sem)
+    g_wide[...] = g_in[...].astype(F32)
+    for h in range(heads):
+        g_lhs[:, h * LANES : (h + 1) * LANES] = g_wide[:, h, :].astype(BF16)
+    branch = jnp.dot(g_lhs[...], wo[...], preferred_element_type=F32).astype(BF16)
+    for t in range(n_tp):
+        b_out[t] = branch[:, t * LANES : (t + 1) * LANES]
+
+    def tp_copy(d):
+        b = lax.rem(tp + d, n_tp)
+        return remote(b_out.at[b], b_in.at[tp], b_sem.at[0, b], b_sem.at[1, tp], (kv, b))
+
+    for d in range(1, n_tp):
+        tp_copy(d).start()
+    b_in[tp] = b_out[tp]
+    for d in range(1, n_tp):
+        b = lax.rem(tp + d, n_tp)
+        remote(b_in.at[b], b_in.at[b], b_sem.at[0, b], b_sem.at[1, b], (kv, b)).wait_recv()
+    residual = (tokens[...].astype(F32) + jnp.sum(b_in[...].astype(F32), 0)).astype(BF16)
+    r_out[...] = residual
+    r_in[me] = residual
+
+    def residual_src(slot):
+        return r_out
+
+    all_send(residual_src, r_in, r_sem)
+    loads[7].wait()
+    loads[8].wait()
+    for j in range(count):
+        cols = slice(j * LANES, (j + 1) * LANES)
+        up_lhs[seqs:, cols] = jnp.where(row == 0, mlp_gain[:, cols], 0.0).astype(BF16)
+    all_recv(r_in, r_sem, 1, count)
+    for j in range(count):
+        cols = slice(j * LANES, (j + 1) * LANES)
+        up_lhs[:seqs, cols] = (r_in[j].astype(F32) * mlp_gain[:, cols]).astype(BF16)
+    mid_average, mid_inverse = moments(r_in[...])
+    lifted = jnp.dot(up_lhs[...], wu[...], preferred_element_type=F32)
+    hidden = jnp.maximum(
+        mid_inverse * (lifted[:seqs] - mid_average * lifted[seqs : seqs + 1]), 0.0
+    )
+    hidden = (hidden * hidden).astype(BF16)
+    per_dot = 8
+    for low in range(0, count, per_dot):
+        high = min(low + per_dot, count)
+        lowered = jnp.dot(
+            hidden, wd[:, low * LANES : high * LANES], preferred_element_type=F32
+        )
+        for j in range(low, high):
+            d_out[j] = lowered[:, (j - low) * LANES : (j - low + 1) * LANES]
+    all_send(lambda slot: d_out.at[slot], d_in, d_sem)
+    d_in[me] = d_out[me]
+
+    all_drain(tokens_src, tok_in, tok_sem)
+    kv_drain(lambda a: q_out.at[a], q_in, q_sem)
+    kv_drain(lambda a: qr_out, qr_in, qr_sem)
+    kv_drain(lambda a: p_out.at[a], p_in, p_sem)
+    kv_drain(lambda a: c_out.at[a], c_in, c_sem)
+    kv_drain(lambda a: g_out, g_in, g_sem)
+    for d in range(1, n_tp):
+        tp_copy(d).wait_send()
+    all_drain(residual_src, r_in, r_sem)
+    all_recv(d_in, d_sem, 1, count)
+    out[...] = (residual.astype(F32) + jnp.sum(d_in[...], 0)).astype(BF16)
+    all_drain(lambda slot: d_out.at[slot], d_in, d_sem)
+
+
+def on_device_fused(n_kv, n_tp, *args):
+    (
+        tokens,
+        lengths,
+        attn_gain,
+        w_query,
+        w_key,
+        w_value,
+        w_gate,
+        decay_rate,
+        key_cache,
+        value_cache,
+        head_gain,
+        w_output,
+        mlp_gain,
+        w_up,
+        w_down,
+    ) = args
+    seqs, block = tokens.shape
+    heads = decay_rate.shape[0]
+    count = n_kv * n_tp
+    fits = (
+        seqs == n_kv
+        and block == LANES
+        and HEAD_VALUE == LANES
+        and heads % 8 == 0
+        and count <= 64
+        and w_output.shape[1] == n_tp * LANES
+    )
+    if not fits:
+        return on_device(*args)
+    half = HEAD_KEY // 2
+    turn_rate = jnp.power(THETA, -jnp.arange(half, dtype=F32) / half)
+    angles = lengths.astype(F32)[:, None] * turn_rate[None, :]
+    cosines = jnp.tile(jnp.cos(angles), (1, LANES // half))
+    sine = jnp.sin(angles)
+    sines = jnp.tile(jnp.concatenate([-sine, sine], 1), (1, LANES // HEAD_KEY))
+    span = key_cache.shape[1]
+    decay = jnp.broadcast_to(decay_rate[:, None], (heads, span))
+    q_rows = w_query.shape[1] // LANES
+    p_rows = q_rows + 2 * heads
+    small = pl.BlockSpec(memory_space=pltpu.VMEM)
+    large = pl.BlockSpec(memory_space=pl.ANY)
+    weights = (
+        w_query, w_key, w_value, w_gate, key_cache, value_cache, w_output, w_up, w_down
+    )
+    vmem = pltpu.VMEM
+    dma = pltpu.SemaphoreType.DMA
+    return pl.pallas_call(
+        functools.partial(layer_kernel, n_kv, n_tp, block * count),
+        out_shape=jax.ShapeDtypeStruct((seqs, block), BF16),
+        in_specs=[pl.BlockSpec(memory_space=pltpu.SMEM)] + [small] * 7 + [large] * 9,
+        out_specs=small,
+        scratch_shapes=[vmem(w.shape, w.dtype) for w in weights]
+        + [
+            vmem((2 * seqs, n_tp * LANES), BF16),
+            vmem((count, seqs, LANES), BF16),
+            vmem((n_kv, q_rows, LANES), F32),
+            vmem((n_kv, q_rows, LANES), F32),
+            vmem((q_rows, LANES), F32),
+            vmem((n_kv, q_rows, LANES), F32),
+            vmem((n_kv, p_rows, LANES), F32),
+            vmem((n_kv, p_rows, LANES), F32),
+            vmem((n_kv, heads, LANES), F32),
+            vmem((n_kv, heads, LANES), F32),
+            vmem((heads, LANES), BF16),
+            vmem((n_kv, heads, LANES), BF16),
+            vmem((n_kv, heads, LANES), F32),
+            vmem((seqs, heads * LANES), BF16),
+            vmem((n_tp, seqs, LANES), BF16),
+            vmem((n_tp, seqs, LANES), BF16),
+            vmem((seqs, LANES), BF16),
+            vmem((count, seqs, LANES), BF16),
+            vmem((2 * seqs, count * LANES), BF16),
+            vmem((count, seqs, LANES), F32),
+            vmem((count, seqs, LANES), F32),
+            dma((len(weights),)),
+            dma((2, count)),
+            dma((2, n_kv)),
+            dma((2, n_kv)),
+            dma((2, n_kv)),
+            dma((2, n_kv)),
+            dma((2, n_kv)),
+            dma((2, n_tp)),
+            dma((2, count)),
+            dma((2, count)),
+        ],
+        compiler_params=pltpu.CompilerParams(
+            collective_id=0, has_side_effects=True, vmem_limit_bytes=56 * 1024 * 1024
+        ),
+    )(
+        lengths,
+        tokens,
+        attn_gain.astype(F32).reshape(1, -1),
+        cosines,
+        sines,
+        decay,
+        head_gain.astype(F32).reshape(heads, LANES),
+        mlp_gain.astype(F32).reshape(1, -1),
+        *weights,
+    )
+
+
 def solution(mesh):
     in_specs = (
         P(None, ("kv", "tp")),
@@ -176,6 +660,7 @@
         P(("kv", "tp"), None),
     )
     out_specs = P(None, ("kv", "tp"))
+    body = functools.partial(on_device_fused, mesh.shape["kv"], mesh.shape["tp"])
     return jax.shard_map(
-        on_device, mesh=mesh, in_specs=in_specs, out_specs=out_specs, check_vma=False
-    )
+        body, mesh=mesh, in_specs=in_specs, out_specs=out_specs, check_vma=False
+    )

time: 388 us -> 67.6 us (0.17)
  waiting for transfers between devices: 206 us -> 0 us
  blocking collectives: 123 us -> 0 us
  Pallas kernels: 0 us -> 58.5 us
  matrix products: 26.8 us -> 0 us
  between operations: 13.3 us -> 0.02 us
  local copies, waits for them, and re-layouts: 8.86 us -> 3.96 us
  other arithmetic: 9.4 us -> 4.66 us
    psum x2 -> x0, waiting for transfers between devices: 123 us -> none  [the longest x1 109 us: on_device(): cached = lax.psum(partial_out, 'kv')]
    reduce_scatter x2 -> x0, waiting for transfers between devices: 79.2 us -> none  [the longest x1 73.3 us: on_device(): lax.psum_scatter(down_terms, 'kv', scatter_dimension=1, tiled=True)]
    psum x1 -> x0, blocking collectives: 78.5 us -> none  [on_device(): lax.psum((part_query, part_key, part_value, part_gate, col_query, col_key...]
    pallas_call x0 -> x1, Pallas kernels: none -> 58.5 us  [on_device_fused(): pl.pallas_call(functools.partial(layer_kernel, n_kv, n_tp, block * count)...]
    all_gather x2 -> x0, blocking collectives: 44.3 us -> none  [the longest x1 42 us: on_device(): lax.all_gather(own_residual, ('kv', 'tp'), axis=1, tiled=True)]
    dot_general x13 -> x0, matrix products: 26.8 us -> none  [the longest x1 6.4 us: on_device(): jnp.einsum('bhj,bjhe->bhe', coefficients, values_local, preferred_element...]
    unnamed x22 -> x1, local copies, waits for them, and re-layouts: 8.69 us -> 1.28 us
    unnamed x6 -> x0, waiting for transfers between devices: 4.02 us -> none
  transfers between devices with their start and end apart: 5 -> 0, of which waited for: 5 -> 0; matrix products, arithmetic and copies ran while one was open for 5% -> 0% of each run, Pallas kernels for 0% -> 0%
where the time goes in v1:
time: 67.6 us; the launch traced here: 67.2 us
  Pallas kernels  58.5 us (87%)
  other arithmetic  4.66 us (7%)
  local copies, waits for them, and re-layouts  3.96 us (6%)
    pallas_call x1, Pallas kernels, on_device_fused(): pl.pallas_call(functools.partial(layer_kernel, n_kv, n_tp, block * count)...  58.5 us

profile of v1, /device:TPU:0, one launch (start us, length us, event | category | flops | bytes accessed | tf_op | source)
XLA Modules:
  0.0 67.2 jit_solution(10062410930446750241)
XLA Ops:
  0.0 0.7 convert_element_type.2
  0.7 0.1 fusion
  0.8 0.1 pad_maximum_fusion
  0.9 0.7 %tile.21.sines = f32[16,128]{1,0:T(8,128)} reshape(f32[16,2,64]{2,1,0:T(2,128)S(1)} %tile.20) | data formatting | bytes 16384 | tf_op jit(solution)/shard_map/tile | solution.py:577
  1.6 0.7 %tile.9.cosines = f32[16,128]{1,0:T(8,128)} reshape(f32[16,4,32]{2,1,0:T(4,128)S(1)} %tile.8) | data formatting | bytes 16384 | tf_op jit(solution)/shard_map/tile | solution.py:575
  2.2 1.3 %reshape.66 = f32[4096]{0:T(1024)} convert(bf16[4096]{0:T(1024)(128)(2,1)} %param.27) | non-fusion elementwise | flops 4096 | bytes 24576 | tf_op jit(solution)/shard_map/reshape | solution.py:639
  3.5 1.3 %bitcast_convert_fusion.head_gain = f32[16,128]{1,0:T(8,128)} fusion(bf16[2048]{0:T(1024)(128)(2,1)} %param.25), kind=kLoop, calls=%fused_computation.3 | loop fusion | flops 2048 | bytes 12288 | tf_op jit(solution)/shard_map/reshape | solution.py:638
  4.8 1.3 %broadcast_in_dim.2.decay = f32[16,128]{1,0:T(8,128)} broadcast(f32[16]{0:T(128)} %param.22), dimensions={0} | broadcast | bytes 8256 | tf_op jit(solution)/shard_map/broadcast_in_dim | solution.py:579
  6.1 1.2 %reshape.62 = f32[256]{0:T(256)} convert(bf16[256]{0:T(256)(128)(2,1)} %param.17) | non-fusion elementwise | flops 256 | bytes 1536 | tf_op jit(solution)/shard_map/reshape | solution.py:634
  7.4 58.5 %shard_map.145 = bf16[16,128]{1,0:T(8,128)(2,1)} custom-call(s32[16]{0:T(128)} %lengths.1, bf16[16,128]{1,0:T(8,128)(2,1)} %tokens.1, f32[1,256]{1,0:T(1,128)} %bitcast.6, f32[16,128]{1,0:T(8,128)} %tile.9.cosines, f32[16,128]{1,0:T(8,128)} %tile.21.sines, f32[16,128]{1,0:T(8,128)} %broadcast_in_dim.2.decay, f32[16,128]{1,0:T(8,128)} %bitcast_convert_fusion.head_gain, ...), custom_call_target="tpu_custom_call" | custom-call | tf_op jit(solution)/shard_map/pallas_call | solution.py:589
  65.9 1.3 %copy.17 = bf16[16,128]{1,0:T(8,128)(2,1)} copy(bf16[16,128]{1,0:T(8,128)(2,1)} %shard_map.145) | data formatting | bytes 8192
  (3 shorter events, 0.0 us)

commit v2 on v1

--- a/solution.py
+++ b/solution.py
@@ -190,11 +190,9 @@
     n_tp,
     width,
     lengths,
+    decay_rate,
     tokens,
     attn_gain,
-    cosines,
-    sines,
-    decay,
     head_gain,
     mlp_gain,
     w_query,
@@ -218,10 +216,13 @@
     wd,
     lhs,
     tok_in,
+    m_out,
+    m_in,
     q_out,
     q_in,
     qr_out,
     qr_in,
+    p_wide,
     p_out,
     p_in,
     c_out,
@@ -239,6 +240,7 @@
     d_in,
     load_sem,
     tok_sem,
+    m_sem,
     q_sem,
     qr_sem,
     p_sem,
@@ -254,7 +256,7 @@
     me = kv * n_tp + tp
     seqs = tokens.shape[0]
     heads = head_gain.shape[0]
-    q_rows = q_out.shape[1]
+    q_rows = q_out.shape[1] // 2
     span = keys.shape[1]
 
     pairs = (
@@ -348,55 +350,97 @@
     def tokens_src(slot):
         return tokens
 
-    all_send(tokens_src, tok_in, tok_sem)
+    def tokens_send(low, high):
+        def body(d, carry):
+            all_copy(tokens_src, tok_in, tok_sem, d).start()
+            return carry
+
+        lax.fori_loop(low, high, body, 0)
+
+    tokens_send(1, n_tp)
     tok_in[me] = tokens[...]
     row = lax.broadcasted_iota(jnp.int32, (seqs, LANES), 0)
     lane = lax.broadcasted_iota(jnp.int32, (seqs, LANES), 1)
-    all_recv(tok_in, tok_sem, 1, n_tp)
+    gains = attn_gain[...].astype(F32)
     for t in range(n_tp):
         cols = slice(t * LANES, (t + 1) * LANES)
-        gain = attn_gain[:, cols]
-        lhs[:seqs, cols] = (tok_in[kv * n_tp + t].astype(F32) * gain).astype(BF16)
-        lhs[seqs:, cols] = jnp.where(row == 0, gain, 0.0).astype(BF16)
+        lhs[seqs:, cols] = jnp.where(row == 0, gains[t : t + 1], 0.0).astype(BF16)
+    all_recv(tok_in, tok_sem, 1, n_tp)
+    first_sum = jnp.zeros((seqs, 1), F32)
+    second_sum = jnp.zeros((seqs, 1), F32)
+    for t in range(n_tp):
+        cols = slice(t * LANES, (t + 1) * LANES)
+        block = tok_in[kv * n_tp + t].astype(F32)
+        lhs[:seqs, cols] = (block * gains[t : t + 1]).astype(BF16)
+        first_sum += jnp.sum(block, -1, keepdims=True)
+        second_sum += jnp.sum(block * block, -1, keepdims=True)
+    m_out[:, 0, :] = jnp.where(lane < LANES // 2, first_sum, second_sum)
     loads[0].wait()
-    first = jnp.dot(lhs[...], wq[...], preferred_element_type=F32)
-    all_recv(tok_in, tok_sem, n_tp, count)
+    product = jnp.dot(lhs[...], wq[...], preferred_element_type=F32)
+    for c in range(q_rows):
+        cols = slice(c * LANES, (c + 1) * LANES)
+        q_out[:, c, :] = product[:seqs, cols]
+        q_out[:, q_rows + c, :] = jnp.broadcast_to(
+            product[seqs : seqs + 1, cols], (seqs, LANES)
+        )
+    kv_send(lambda a: m_out.at[a], m_in, m_sem)
+    kv_send(lambda a: q_out.at[a], q_in, q_sem)
+    tokens_send(n_tp, count)
+    m_in[kv] = m_out[kv]
+    q_in[kv] = q_out[kv]
+
+    lane_row = lax.broadcasted_iota(jnp.int32, (1, LANES), 1)
+    half = HEAD_KEY // 2
+    turn_rate = jnp.zeros((1, LANES), F32)
+    for i in range(half):
+        turn_rate = jnp.where(lane_row % half == i, THETA ** (-i / half), turn_rate)
+    angle = lengths[kv].astype(F32) * turn_rate
+    cosine = jnp.cos(angle)
+    sine = jnp.sin(angle)
+    sine = jnp.where(lane_row % HEAD_KEY < half, -sine, sine)
+    decay = jnp.zeros((heads, LANES), F32)
+    for h in range(heads):
+        decay = jnp.where(
+            lax.broadcasted_iota(jnp.int32, (heads, LANES), 0) == h, decay_rate[h], decay
+        )
+
+    def normalizer(first, second):
+        average = first / width
+        return average, lax.rsqrt(second / width - average * average + EPS)
 
     def moments(blocks):
         wide = blocks.astype(F32)
-        average = jnp.sum(jnp.sum(wide, 0), -1, keepdims=True) / width
-        square = jnp.sum(jnp.sum(wide * wide, 0), -1, keepdims=True) / width
-        return average, lax.rsqrt(square - average * average + EPS)
-
+        return normalizer(
+            jnp.sum(jnp.sum(wide, 0), -1, keepdims=True),
+            jnp.sum(jnp.sum(wide * wide, 0), -1, keepdims=True),
+        )
+
+    kv_recv(m_in, m_sem)
+    sums = jnp.sum(m_in[...], 0)
+    own_average, own_inverse = normalizer(sums[:, :1], sums[:, LANES - 1 :])
+    kv_recv(q_in, q_sem)
+    total = jnp.sum(q_in[...], 0)
+    query = own_inverse * (total[:q_rows] - own_average * total[q_rows:])
+    query = turn(query, cosine, sine).astype(BF16)
+    qr_out[...] = query
+    qr_in[kv] = query
+    query = query.astype(F32)
+    kv_send(lambda a: qr_out, qr_in, qr_sem)
+
+    all_recv(tok_in, tok_sem, n_tp, count)
     average, inverse = moments(tok_in[...])
-
-    def spread(product, dst, base):
-        part = inverse * (product[:seqs] - average * product[seqs : seqs + 1])
-        for c in range(part.shape[1] // LANES):
-            dst[:, base + c, :] = part[:, c * LANES : (c + 1) * LANES]
-
-    spread(first, q_out, 0)
-    kv_send(lambda a: q_out.at[a], q_in, q_sem)
-    q_in[kv] = q_out[kv]
-
     base = 0
     for which, weight in ((1, wk), (2, wv), (3, wg)):
         loads[which].wait()
         for low in range(0, weight.shape[1], 1024):
             high = min(low + 1024, weight.shape[1])
-            spread(
-                jnp.dot(lhs[...], weight[:, low:high], preferred_element_type=F32), p_out, base
-            )
+            product = jnp.dot(lhs[...], weight[:, low:high], preferred_element_type=F32)
+            part = inverse * (product[:seqs] - average * product[seqs : seqs + 1])
+            for c in range(part.shape[1] // LANES):
+                p_wide[:, base + c, :] = part[:, c * LANES : (c + 1) * LANES]
             base += (high - low) // LANES
+    p_out[...] = p_wide[...].astype(BF16)
     p_in[kv] = p_out[kv]
-
-    cosine = cosines[pl.ds(kv, 1), :]
-    sine = sines[pl.ds(kv, 1), :]
-    kv_recv(q_in, q_sem)
-    query = turn(jnp.sum(q_in[...], 0), cosine, sine).astype(BF16).astype(F32)
-    qr_out[...] = query
-    qr_in[kv] = query
-    kv_send(lambda a: qr_out, qr_in, qr_sem)
     kv_send(lambda a: p_out.at[a], p_in, p_sem)
 
     loads[4].wait()
@@ -407,42 +451,48 @@
     head_lane = lax.broadcasted_iota(jnp.int32, (heads, LANES), 1)
     place = kv * span + lax.broadcasted_iota(jnp.int32, (1, span), 1)
 
-    def attend(i, carry):
-        s = lax.rem(kv + 1 + i, n_kv)
-        rows = qr_in[s]
-        pieces = [
-            jnp.where(
-                head_row == per_row * r + head_lane // HEAD_KEY,
-                jnp.broadcast_to(rows[r : r + 1], (heads, LANES)),
-                0.0,
-            )
-            for r in range(q_rows)
-        ]
-        blocked = jnp.concatenate(pieces, 1).astype(BF16)
-        scores = lax.dot_general(
-            blocked, keys[s], (((1,), (1,)), ((), ())), preferred_element_type=F32
-        ) * HEAD_KEY ** (-0.5)
-        length = lengths[s]
-        distance = jnp.maximum(length - place, 0).astype(F32)
-        fade = jnp.where(place < length, jnp.exp(-decay[...] * distance), 0.0)
-        coefficients = (scores * fade).astype(BF16)
-        mixed = jnp.dot(coefficients, values[s], preferred_element_type=F32)
-        kept = jnp.zeros((heads, LANES), F32)
-        for h in range(heads):
-            kept = jnp.where(head_row == h, mixed[:, h * LANES : (h + 1) * LANES], kept)
-        c_out[s] = kept
-
-        @pl.when(i < n_kv - 1)
-        def _():
-            kv_copy(lambda a: c_out.at[a], c_in, c_sem, 1 + i).start()
+    group = 4 if n_kv % 4 == 0 else 1
+    where_lane = [head_row == per_row * r + head_lane // HEAD_KEY for r in range(q_rows)]
+
+    def attend(step, carry):
+        order = [lax.rem(kv + 1 + step * group + k, n_kv) for k in range(group)]
+        coefficients = []
+        for s in order:
+            rows = qr_in[s].astype(F32)
+            pieces = [
+                jnp.where(
+                    where_lane[r], jnp.broadcast_to(rows[r : r + 1], (heads, LANES)), 0.0
+                )
+                for r in range(q_rows)
+            ]
+            blocked = jnp.concatenate(pieces, 1).astype(BF16)
+            scores = lax.dot_general(
+                blocked, keys[s], (((1,), (1,)), ((), ())), preferred_element_type=F32
+            ) * HEAD_KEY ** (-0.5)
+            length = lengths[s]
+            distance = jnp.maximum(length - place, 0).astype(F32)
+            fade = jnp.where(place < length, jnp.exp(-decay[:, :1] * distance), 0.0)
+            coefficients.append((scores * fade).astype(BF16))
+        for s, coefficient in zip(order, coefficients):
+            mixed = jnp.dot(coefficient, values[s], preferred_element_type=F32)
+            kept = jnp.zeros((heads, LANES), F32)
+            for h in range(heads):
+                kept = jnp.where(head_row == h, mixed[:, h * LANES : (h + 1) * LANES], kept)
+            c_out[s] = kept.astype(BF16)
+        for k in range(group):
+            d = 1 + step * group + k
+
+            @pl.when(d < n_kv)
+            def _():
+                kv_copy(lambda a: c_out.at[a], c_in, c_sem, d).start()
 
         return carry
 
-    lax.fori_loop(0, n_kv, attend, 0)
+    lax.fori_loop(0, n_kv // group, attend, 0)
     c_in[kv] = c_out[kv]
 
     kv_recv(p_in, p_sem)
-    totals = jnp.sum(p_in[...], 0)
+    totals = jnp.sum(p_in[...].astype(F32), 0)
     fresh_key = turn(totals[:q_rows], cosine, sine).astype(BF16).astype(F32)
     fresh_value = totals[q_rows : q_rows + heads].astype(BF16).astype(F32)
     gate = totals[q_rows + heads :]
@@ -459,12 +509,12 @@
     gate = gate * jax.nn.sigmoid(gate)
 
     kv_recv(c_in, c_sem)
-    retained = jnp.sum(c_in[...], 0) + addend
+    retained = jnp.sum(c_in[...].astype(F32), 0) + addend
     centered = retained - jnp.mean(retained, -1, keepdims=True)
     normed = (
         centered
         * lax.rsqrt(jnp.mean(centered * centered, -1, keepdims=True) + EPS)
-        * head_gain[...]
+        * head_gain[...].astype(F32)
     )
     gated = (gate * normed).astype(BF16)
     g_out[...] = gated
@@ -500,31 +550,45 @@
     all_send(residual_src, r_in, r_sem)
     loads[7].wait()
     loads[8].wait()
+    gains = mlp_gain[...].astype(F32)
     for j in range(count):
         cols = slice(j * LANES, (j + 1) * LANES)
-        up_lhs[seqs:, cols] = jnp.where(row == 0, mlp_gain[:, cols], 0.0).astype(BF16)
+        up_lhs[seqs:, cols] = jnp.where(row == 0, gains[j : j + 1], 0.0).astype(BF16)
     all_recv(r_in, r_sem, 1, count)
     for j in range(count):
         cols = slice(j * LANES, (j + 1) * LANES)
-        up_lhs[:seqs, cols] = (r_in[j].astype(F32) * mlp_gain[:, cols]).astype(BF16)
+        up_lhs[:seqs, cols] = (r_in[j].astype(F32) * gains[j : j + 1]).astype(BF16)
     mid_average, mid_inverse = moments(r_in[...])
     lifted = jnp.dot(up_lhs[...], wu[...], preferred_element_type=F32)
     hidden = jnp.maximum(
         mid_inverse * (lifted[:seqs] - mid_average * lifted[seqs : seqs + 1]), 0.0
     )
     hidden = (hidden * hidden).astype(BF16)
-    per_dot = 8
-    for low in range(0, count, per_dot):
-        high = min(low + per_dot, count)
-        lowered = jnp.dot(
-            hidden, wd[:, low * LANES : high * LANES], preferred_element_type=F32
-        )
-        for j in range(low, high):
-            d_out[j] = lowered[:, (j - low) * LANES : (j - low + 1) * LANES]
-    all_send(lambda slot: d_out.at[slot], d_in, d_sem)
+    per_dot = 8 if count % 8 == 0 else 1
+    chunks = count // per_dot
+    for i in range(chunks):
+        low = lax.rem(me // per_dot + 1 + i, chunks) * per_dot
+        cols = pl.ds(pl.multiple_of(low * LANES, LANES * per_dot), LANES * per_dot)
+        lowered = jnp.dot(hidden, wd[:, cols], preferred_element_type=F32)
+        for k in range(per_dot):
+            d_out[low + k] = lowered[:, k * LANES : (k + 1) * LANES].astype(BF16)
+        for k in range(per_dot):
+            slot = low + lax.rem(me + k, per_dot)
+
+            @pl.when(slot != me)
+            def _():
+                remote(
+                    d_out.at[slot],
+                    d_in.at[me],
+                    d_sem.at[0, slot],
+                    d_sem.at[1, me],
+                    (slot // n_tp, lax.rem(slot, n_tp)),
+                ).start()
+
     d_in[me] = d_out[me]
 
     all_drain(tokens_src, tok_in, tok_sem)
+    kv_drain(lambda a: m_out.at[a], m_in, m_sem)
     kv_drain(lambda a: q_out.at[a], q_in, q_sem)
     kv_drain(lambda a: qr_out, qr_in, qr_sem)
     kv_drain(lambda a: p_out.at[a], p_in, p_sem)
@@ -534,7 +598,7 @@
         tp_copy(d).wait_send()
     all_drain(residual_src, r_in, r_sem)
     all_recv(d_in, d_sem, 1, count)
-    out[...] = (residual.astype(F32) + jnp.sum(d_in[...], 0)).astype(BF16)
+    out[...] = (residual.astype(F32) + jnp.sum(d_in[...].astype(F32), 0)).astype(BF16)
     all_drain(lambda slot: d_out.at[slot], d_in, d_sem)
 
 
@@ -569,14 +633,6 @@
     )
     if not fits:
         return on_device(*args)
-    half = HEAD_KEY // 2
-    turn_rate = jnp.power(THETA, -jnp.arange(half, dtype=F32) / half)
-    angles = lengths.astype(F32)[:, None] * turn_rate[None, :]
-    cosines = jnp.tile(jnp.cos(angles), (1, LANES // half))
-    sine = jnp.sin(angles)
-    sines = jnp.tile(jnp.concatenate([-sine, sine], 1), (1, LANES // HEAD_KEY))
-    span = key_cache.shape[1]
-    decay = jnp.broadcast_to(decay_rate[:, None], (heads, span))
     q_rows = w_query.shape[1] // LANES
     p_rows = q_rows + 2 * heads
     small = pl.BlockSpec(memory_space=pltpu.VMEM)
@@ -589,20 +645,23 @@
     return pl.pallas_call(
         functools.partial(layer_kernel, n_kv, n_tp, block * count),
         out_shape=jax.ShapeDtypeStruct((seqs, block), BF16),
-        in_specs=[pl.BlockSpec(memory_space=pltpu.SMEM)] + [small] * 7 + [large] * 9,
+        in_specs=[pl.BlockSpec(memory_space=pltpu.SMEM)] * 2 + [small] * 4 + [large] * 9,
         out_specs=small,
         scratch_shapes=[vmem(w.shape, w.dtype) for w in weights]
         + [
             vmem((2 * seqs, n_tp * LANES), BF16),
             vmem((count, seqs, LANES), BF16),
-            vmem((n_kv, q_rows, LANES), F32),
-            vmem((n_kv, q_rows, LANES), F32),
-            vmem((q_rows, LANES), F32),
-            vmem((n_kv, q_rows, LANES), F32),
+            vmem((n_kv, 1, LANES), F32),
+            vmem((n_kv, 1, LANES), F32),
+            vmem((n_kv, 2 * q_rows, LANES), F32),
+            vmem((n_kv, 2 * q_rows, LANES), F32),
+            vmem((q_rows, LANES), BF16),
+            vmem((n_kv, q_rows, LANES), BF16),
             vmem((n_kv, p_rows, LANES), F32),
-            vmem((n_kv, p_rows, LANES), F32),
-            vmem((n_kv, heads, LANES), F32),
-            vmem((n_kv, heads, LANES), F32),
+            vmem((n_kv, p_rows, LANES), BF16),
+            vmem((n_kv, p_rows, LANES), BF16),
+            vmem((n_kv, heads, LANES), BF16),
+            vmem((n_kv, heads, LANES), BF16),
             vmem((heads, LANES), BF16),
             vmem((n_kv, heads, LANES), BF16),
             vmem((n_kv, heads, LANES), F32),
@@ -612,10 +671,11 @@
             vmem((seqs, LANES), BF16),
             vmem((count, seqs, LANES), BF16),
             vmem((2 * seqs, count * LANES), BF16),
-            vmem((count, seqs, LANES), F32),
-            vmem((count, seqs, LANES), F32),
+            vmem((count, seqs, LANES), BF16),
+            vmem((count, seqs, LANES), BF16),
             dma((len(weights),)),
             dma((2, count)),
+            dma((2, n_kv)),
             dma((2, n_kv)),
             dma((2, n_kv)),
             dma((2, n_kv)),
@@ -630,13 +690,11 @@
         ),
     )(
         lengths,
+        decay_rate,
         tokens,
-        attn_gain.astype(F32).reshape(1, -1),
-        cosines,
-        sines,
-        decay,
-        head_gain.astype(F32).reshape(heads, LANES),
-        mlp_gain.astype(F32).reshape(1, -1),
+        attn_gain.reshape(n_tp, LANES),
+        head_gain.reshape(heads, LANES),
+        mlp_gain.reshape(count, LANES),
         *weights,
     )
 

time: 67.6 us -> 51.4 us (0.76)
  Pallas kernels: 58.5 us -> 49.9 us
  other arithmetic: 4.66 us -> 0 us
  local copies, waits for them, and re-layouts: 3.96 us -> 1.28 us
    pallas_call x1, Pallas kernels: 58.5 us -> 49.9 us  [on_device_fused(): pl.pallas_call(functools.partial(layer_kernel, n_kv, n_tp, block * count)...]
    reshape x3 -> x0, other arithmetic: 3.8 us -> none  [the longest x1 1.3 us: on_device_fused(): mlp_gain.astype(F32).reshape(1, -1)]
    another operation x4 -> x0, local copies, waits for them, and re-layouts: 1.36 us -> none  [the longest x2 0.68 us: on_device_fused(): sines = jnp.tile(jnp.concatenate([-sine, sine], 1), (1, LANES // HEAD_KEY))]
    broadcast_in_dim x1 -> x0, local copies, waits for them, and re-layouts: 1.32 us -> none  [on_device_fused(): decay = jnp.broadcast_to(decay_rate[:, None], (heads, span))]
where the time goes in v2:
time: 51.4 us; the launch traced here: 51.2 us
  Pallas kernels  49.9 us (97%)
  local copies, waits for them, and re-layouts  1.28 us (2%)
    pallas_call x1, Pallas kernels, on_device_fused(): pl.pallas_call(functools.partial(layer_kernel, n_kv, n_tp, block * count)...  49.9 us
    unnamed x1, local copies, waits for them, and re-layouts  1.28 us

profile of v2, /device:TPU:0, one launch (start us, length us, event | category | flops | bytes accessed | tf_op | source)
XLA Modules:
  0.0 51.2 jit_solution(326334340691923236)
XLA Ops:
  0.0 49.9 %shard_map.145 = bf16[16,128]{1,0:T(8,128)(2,1)} custom-call(s32[16]{0:T(128)} %lengths.1, f32[16]{0:T(128)} %decay_rate.1, bf16[16,128]{1,0:T(8,128)(2,1)} %tokens.1, bf16[2,128]{1,0:T(2,128)(2,1)} %bitcast.5, bf16[16,128]{1,0:T(8,128)(2,1)} %bitcast.4, bf16[32,128]{1,0:T(8,128)(2,1)} %bitcast.3, bf16[256,1024]{1,0:T(8,128)(2,1)} %w_query.1, ...), custom_call_target="tpu_custom_call" | custom-call | tf_op jit(solution)/shard_map/pallas_call | solution.py:645
  49.9 1.3 %copy.17 = bf16[16,128]{1,0:T(8,128)(2,1)} copy(bf16[16,128]{1,0:T(8,128)(2,1)} %shard_map.145) | data formatting | bytes 8192
